TPU v7x, 32 devices: a whole 2x2x4 slice. The times are simulated.
32 devices in a mesh: sp: 8 (over z, y), tp: 4 (over x, core).
Axes of the slice: x: 2, y: 2, z: 4, core: 2. Of those that a mesh axis runs over, the one named last changes fastest.
Arguments:
- resid_in: bfloat16 [2048, 2048], P('sp'), may hold values from -6 to 6
- query_latent: bfloat16 [2048, 768], P('sp'), may hold values from -6 to 6
- kv_latent: bfloat16 [2048, 512], P('sp'), may hold values from -6 to 6
- rotary_key: bfloat16 [2048, 64], P('sp'), may hold values from -200 to 200
- query_gain: float32 [768], replicated, may hold values from 0.1 to 1.9
- kv_gain: float32 [512], replicated, may hold values from 0.1 to 1.9
- w_query_plain: bfloat16 [768, 2048], P(None, 'tp'), may hold values from -0.875 to 0.875
- w_query_rotary: bfloat16 [768, 1024], P(None, 'tp'), may hold values from -0.875 to 0.875
- w_key_plain: bfloat16 [512, 2048], P(None, 'tp'), may hold values from -0.25 to 0.25
- w_value: bfloat16 [512, 2048], P(None, 'tp'), may hold values from -0.25 to 0.25
- w_output: bfloat16 [2048, 2048], P('tp'), may hold values from -0.125 to 0.125
- ffn_gain: float32 [2048], replicated, may hold values from 0.1 to 1.9
- w_gate: bfloat16 [2048, 5632], P('sp', 'tp'), may hold values from -0.125 to 0.125
- w_up: bfloat16 [2048, 5632], P('sp', 'tp'), may hold values from -0.125 to 0.125
- w_down: bfloat16 [5632, 2048], P('tp', 'sp'), may hold values from -0.078125 to 0.078125
Outputs:
- resid_out: bfloat16 [2048, 2048], P(('sp', 'tp'))
All inputs are finite; a program needn't handle non-finite values.
Results may differ from a plain program's by a relative error of at most 0.014.
The roundings to bfloat16 on the way count: a program that leaves them out, or rounds other values in their place, can miss the bound.
Values may be sent and summed in bfloat16 or wider, within the bound.
A program may use at most 192 MiB of HBM per device.

v0:
```python
import functools

import jax
import jax.numpy as jnp
from jax import lax
from jax.experimental import pallas as pl
from jax.experimental.pallas import tpu as pltpu
from jax.sharding import PartitionSpec as P

NOPE = 128
ROPE = 64
VDIM = 128
MESH = pl.DeviceIdType.MESH


def normed(values, gain):
    wide = values.astype(jnp.float32)
    return wide * lax.rsqrt(jnp.mean(wide * wide, axis=-1, keepdims=True) + 1e-06) * gain


def rotate(values, cosine, sine):
    half = values.shape[-1] // 2
    first = values[..., :half]
    second = values[..., half:]
    return jnp.concatenate(
        [first * cosine - second * sine, second * cosine + first * sine], axis=-1
    )


class Plan:
    def __init__(self, sp, tp):
        self.sp, self.tp = sp, tp
        self.z = 4 if sp % 4 == 0 else 1
        self.r = sp // self.z
        self.c = 2 if tp % 2 == 0 else 1
        self.x = tp // self.c

    def sizes(self):
        return {"z": self.z, "r": self.r, "x": self.x, "c": self.c}

    def here(self):
        s, t = lax.axis_index("sp"), lax.axis_index("tp")
        return {"z": s // self.r, "r": lax.rem(s, self.r), "x": t // self.c, "c": lax.rem(t, self.c)}

    def device(self, at):
        return {"sp": at["z"] * self.r + at["r"], "tp": at["x"] * self.c + at["c"]}

    def shifted(self, at, axis, by):
        size = self.sizes()[axis]
        return {**at, axis: lax.rem(at[axis] + (by % size), size)}


def meet(plan, here, axes):
    barrier = pltpu.get_barrier_semaphore()
    count = 0
    for axis in axes:
        for k in range(1, plan.sizes()[axis]):
            pl.semaphore_signal(
                barrier,
                inc=1,
                device_id=plan.device(plan.shifted(here, axis, k)),
                device_id_type=MESH,
            )
            count += 1
    if count:
        pl.semaphore_wait(barrier, count)


def front_body(
    plan,
    heads,
    part,
    kv_ref,
    qp_ref,
    qr_ref,
    wk_ref,
    wv_ref,
    wo_ref,
    resid_ref,
    gain_ref,
    gate_ref,
    up_ref,
    down_ref,
    mid_ref,
    hn_ref,
    both_ref,
    downs_ref,
    packed,
    attn,
    out,
    terms,
    h_own,
    kv_sa,
    kv_ra,
    kv_sb,
    kv_rb,
    kv_sc,
    kv_rc,
    hn_sa,
    hn_ra,
    hn_sb,
    hn_rb,
    hn_sc,
    hn_rc,
    w_sa,
    w_ra,
    w_sb,
    w_rb,
    t_s,
    t_r,
    local,
):
    here = plan.here()
    sizes = plan.sizes()
    nz, nr, tp = plan.z, plan.r, plan.tp
    latent = wk_ref.shape[0]
    depth, full = gate_ref.shape
    narrow = down_ref.shape[1]
    sp_here, tp_here = lax.axis_index("sp"), lax.axis_index("tp")

    barrier = pltpu.get_barrier_semaphore()
    peers = [plan.shifted(here, "z", k) for k in range(1, nz)]
    peers += [plan.shifted(here, "r", k) for k in range(1, nr)]
    peers = [plan.device(at) for at in peers]
    peers += [{"sp": sp_here, "tp": lax.rem(tp_here + k, tp)} for k in range(1, tp)]
    for peer in peers:
        pl.semaphore_signal(barrier, inc=1, device_id=peer, device_id_type=MESH)
    pl.semaphore_wait(barrier, len(peers))

    def send(src, dst, device, sem_s, sem_r):
        copy = pltpu.make_async_remote_copy(
            src_ref=src,
            dst_ref=dst,
            send_sem=sem_s,
            recv_sem=sem_r,
            device_id=device,
            device_id_type=MESH,
        )
        copy.start()
        return copy

    class Gather:
        def __init__(self, axes, x_ref, o_ref, sems, own):
            self.axes, self.x_ref, self.o_ref, self.sems = axes, x_ref, o_ref, sems
            self.copies = {}
            self.mine = pltpu.make_async_copy(x_ref, o_ref.at[self.slot(here)], own)

        def slot(self, at):
            index = 0
            for axis in self.axes:
                index = index * sizes[axis] + at[axis]
            return index

        def send(self, stage, block, by, key):
            mine = len(key) == 0 or not any(key)
            src = self.x_ref if mine else self.o_ref.at[self.slot(block)]
            sem_s, sem_r = self.sems[2 * stage], self.sems[2 * stage + 1]
            at = (key + (by,)) if stage else by
            self.copies[key + (by,)] = send(
                src,
                self.o_ref.at[self.slot(block)],
                plan.device(plan.shifted(here, self.axes[stage], by)),
                sem_s.at[at],
                sem_r.at[at],
            )

        def start(self):
            self.mine.start()
            for k in range(1, sizes[self.axes[0]]):
                self.send(0, here, k, ())

        def run(self):
            na, nb, nc = (sizes[axis] for axis in self.axes)
            for k in range(na):
                block = plan.shifted(here, self.axes[0], -k)
                if k:
                    self.copies[(k,)].wait_recv()
                for j in range(1, nb):
                    self.send(1, block, j, (k,))
                for l in range(1, nc):
                    self.send(2, block, l, (k, 0))
            for k in range(na):
                for j in range(1, nb):
                    self.copies[(k, j)].wait_recv()
                    block = plan.shifted(here, self.axes[0], -k)
                    block = plan.shifted(block, self.axes[1], -j)
                    for l in range(1, nc):
                        self.send(2, block, l, (k, j))

        def finish(self):
            for key, copy in self.copies.items():
                if len(key) == 3:
                    copy.wait_recv()
            for copy in self.copies.values():
                copy.wait_send()
            self.mine.wait()

    def window(index):
        return pl.multiple_of(jnp.minimum(index * part, full - part), 128)

    def targets(sp):
        rows = pl.ds(pl.multiple_of(sp * depth, depth), depth)
        if len(downs_ref.shape) == 3:
            downs = downs_ref.at[sp]
        else:
            downs = downs_ref.at[:, pl.ds(pl.multiple_of(sp * narrow, 128), narrow)]
        return [
            both_ref.at[rows, pl.ds(0, part)],
            both_ref.at[rows, pl.ds(part, part)],
            downs,
        ]

    def sources(index):
        lanes = pl.ds(window(index), part)
        return [gate_ref.at[:, lanes], up_ref.at[:, lanes], down_ref.at[lanes, :]]

    kv = Gather(("z", "r", "c"), kv_ref, packed, (kv_sa, kv_ra, kv_sb, kv_rb, kv_sc, kv_rc), local.at[0])
    kv.start()
    over_z, over_r = {}, {}
    mine = []
    for w in range(3):
        src, dst = sources(here["z"])[w], targets(sp_here)[w]
        mine.append(pltpu.make_async_copy(src, dst, local.at[2 + w]))
        mine[-1].start()
        for k in range(1, nz):
            to = plan.shifted(here, "z", k)
            over_z[w, k] = send(
                sources(to["z"])[w], dst, plan.device(to), w_sa.at[w, k], w_ra.at[w, k]
            )
    kv.run()

    def forward(w, k):
        block = plan.shifted(here, "z", -k)
        dst = targets(block["z"] * nr + here["r"])[w]
        src = dst if k else sources(here["z"])[w]
        if k:
            over_z[w, k].wait_recv()
        for j in range(1, nr):
            over_r[w, k, j] = send(
                src,
                dst,
                plan.device(plan.shifted(here, "r", j)),
                w_sb.at[w, k, j],
                w_rb.at[w, k, j],
            )

    for w in range(3):
        forward(w, 0)
    kv.finish()

    scale = (NOPE + ROPE) ** (-0.5)
    count = packed.shape[0] * packed.shape[1]

    def transposed(left, right):
        return lax.dot_general(
            left, right, (((1,), (1,)), ((), ())), preferred_element_type=jnp.float32
        )

    @pl.loop(0, heads)
    def _(h):
        lanes = pl.ds(pl.multiple_of(h * NOPE, NOPE), NOPE)
        lat = packed[:, :, :latent].reshape(count, latent)
        rot = packed[:, :, latent:].reshape(count, ROPE)
        keys = jnp.dot(lat, wk_ref[:, lanes], preferred_element_type=jnp.float32)
        vals = jnp.dot(lat, wv_ref[:, lanes], preferred_element_type=jnp.float32)
        keys, vals = keys.astype(jnp.bfloat16), vals.astype(jnp.bfloat16)
        score = (transposed(qp_ref[:, lanes], keys) + transposed(qr_ref[h], rot)) * scale
        weight = jnp.exp(score - jnp.max(score, axis=-1, keepdims=True))
        total = jnp.sum(weight, axis=-1, keepdims=True)
        mixed = jnp.dot(weight.astype(jnp.bfloat16), vals, preferred_element_type=jnp.float32)
        attn[:, lanes] = (mixed / total).astype(jnp.bfloat16)

    share = out.shape[1]
    swaps = []
    for k in list(range(1, tp)) + [0]:
        to = lax.rem(tp_here + k, tp)
        rows = pl.ds(pl.multiple_of(to * share, share), share)
        out[to] = jnp.dot(
            attn[rows, :], wo_ref[...], preferred_element_type=jnp.float32
        ).astype(jnp.bfloat16)
        if k:
            swaps.append(
                send(out.at[to], terms.at[k], {"sp": sp_here, "tp": to}, t_s.at[k], t_r.at[k])
            )
    for w in range(2):
        for k in range(1, nz):
            forward(w, k)
    mid = resid_ref[...].astype(jnp.float32) + out[tp_here].astype(jnp.float32)
    for k, copy in enumerate(swaps, 1):
        copy.wait_recv()
        mid += terms[k].astype(jnp.float32)
    mid_ref[...] = mid
    h_own[...] = (
        mid * lax.rsqrt(jnp.mean(mid * mid, axis=-1, keepdims=True) + 1e-06) * gain_ref[...]
    ).astype(jnp.bfloat16)
    hn = Gather(("z", "x", "c"), h_own, hn_ref, (hn_sa, hn_ra, hn_sb, hn_rb, hn_sc, hn_rc), local.at[1])
    hn.start()
    for k in range(1, nz):
        forward(2, k)
    hn.run()
    hn.finish()
    for copy in swaps:
        copy.wait_send()
    for copy in over_r.values():
        copy.wait_recv()
    for copy in [*over_z.values(), *over_r.values()]:
        copy.wait_send()
    for copy in mine:
        copy.wait()


def front(plan, heads, part, kv, qp, qr, wk, wv, wo, resid, gain, gate, up, down, ident):
    nz, nr, nx, nc, tp = plan.z, plan.r, plan.x, plan.c, plan.tp
    share, width = resid.shape
    tok = qp.shape[0]
    dma = pltpu.SemaphoreType.DMA
    vmem = pl.BlockSpec(memory_space=pltpu.VMEM)
    hbm = pl.BlockSpec(memory_space=pl.ANY)

    def sems(a, b, c):
        return [dma((a,)), dma((a,)), dma((a, b)), dma((a, b)), dma((a, b, c)), dma((a, b, c))]

    bf = jnp.bfloat16
    narrow = down.shape[1]
    downs = (part, plan.sp * narrow) if narrow % 128 == 0 else (plan.sp, part, narrow)
    return pl.pallas_call(
        functools.partial(front_body, plan, heads, part),
        out_shape=(
            jax.ShapeDtypeStruct((share, width), jnp.float32),
            jax.ShapeDtypeStruct((nz * tp, share, width), bf),
            jax.ShapeDtypeStruct((plan.sp * gate.shape[0], 2 * part), bf),
            jax.ShapeDtypeStruct(downs, bf),
        ),
        in_specs=[vmem] * 11,
        out_specs=(vmem, hbm, hbm, hbm),
        scratch_shapes=[
            pltpu.VMEM((nz * nr * nc,) + kv.shape, bf),
            pltpu.VMEM((tok, heads * VDIM), bf),
            pltpu.VMEM((tp, share, width), bf),
            pltpu.VMEM((tp, share, width), bf),
            pltpu.VMEM((share, width), bf),
            *sems(nz, nr, nc),
            *sems(nz, nx, nc),
            dma((3, nz)),
            dma((3, nz)),
            dma((3, nz, nr)),
            dma((3, nz, nr)),
            dma((tp,)),
            dma((tp,)),
            dma((5,)),
        ],
        compiler_params=pltpu.CompilerParams(
            collective_id=ident, has_side_effects=True, vmem_limit_bytes=56 * 1024 * 1024
        ),
    )(kv, qp, qr, wk, wv, wo, resid, gain, gate, up, down)


def reduce_body(
    plan, p_ref, m_ref, o_ref, got_c, sum_c, got_x, sum_x, got_z, s_c, r_c, s_x, r_x, s_z, r_z
):
    nz, nx, nc = plan.z, plan.x, plan.c
    here = plan.here()
    z, x, c = here["z"], here["x"], here["c"]
    meet(plan, here, ("z", "x", "c"))

    def send(src, dst, axis, by, sem_s, sem_r):
        copy = pltpu.make_async_remote_copy(
            src_ref=src,
            dst_ref=dst,
            send_sem=sem_s,
            recv_sem=sem_r,
            device_id=plan.device(plan.shifted(here, axis, by)),
            device_id_type=MESH,
        )
        copy.start()
        return copy

    def wide(value):
        return value.astype(jnp.float32)

    steps = [k for k in (2, 1, 3) if k < nz] + [0]
    if nz != 4:
        steps = list(range(1, nz)) + [0]
    over_c, over_x, over_z = {}, {}, {}
    for k in steps:
        to = lax.rem(z + k, nz)
        for l in range(1, nc):
            other = lax.rem(c + l, nc)
            for i in range(nx):
                over_c[k, i, l] = send(
                    p_ref.at[to, i, other],
                    got_c.at[k, i, l - 1],
                    "c",
                    l,
                    s_c.at[k, i, l],
                    r_c.at[k, i, l],
                )

    def fold_c(k):
        to = lax.rem(z + k, nz)
        for i in range(nx):
            total = wide(p_ref[to, i, c])
            for l in range(1, nc):
                over_c[k, i, l].wait_recv()
                total += wide(got_c[k, i, l - 1])
            sum_c[k, i] = total.astype(jnp.bfloat16)
        for j in range(1, nx):
            over_x[k, j] = send(
                sum_c.at[k, lax.rem(x + j, nx)],
                got_x.at[k, j - 1],
                "x",
                j,
                s_x.at[k, j],
                r_x.at[k, j],
            )

    def fold_x(k):
        total = wide(sum_c[k, x])
        for j in range(1, nx):
            over_x[k, j].wait_recv()
            total += wide(got_x[k, j - 1])
        if k:
            sum_x[k - 1] = total.astype(jnp.bfloat16)
            over_z[k] = send(sum_x.at[k - 1], got_z.at[k - 1], "z", k, s_z.at[k], r_z.at[k])
            return None
        return total

    for k in steps:
        fold_c(k)
    for k in steps:
        total = fold_x(k)
    for k in steps:
        if k:
            over_z[k].wait_recv()
            total += wide(got_z[k - 1])
    o_ref[...] = (m_ref[...] + total).astype(jnp.bfloat16)
    for copy in [*over_c.values(), *over_x.values(), *over_z.values()]:
        copy.wait_send()


def reduce_add(plan, partial, mid, ident):
    nz, nx, nc = plan.z, plan.x, plan.c
    rows, width = mid.shape
    dma = pltpu.SemaphoreType.DMA

    def buf(*lead):
        return pltpu.VMEM(lead + (rows, width), jnp.bfloat16)

    vmem = pl.BlockSpec(memory_space=pltpu.VMEM)
    return pl.pallas_call(
        functools.partial(reduce_body, plan),
        out_shape=jax.ShapeDtypeStruct(mid.shape, jnp.bfloat16),
        in_specs=[vmem, vmem],
        out_specs=vmem,
        scratch_shapes=[
            buf(nz, nx, max(nc - 1, 1)),
            buf(nz, nx),
            buf(nz, max(nx - 1, 1)),
            buf(max(nz - 1, 1)),
            buf(max(nz - 1, 1)),
            dma((nz, nx, nc)),
            dma((nz, nx, nc)),
            dma((nz, nx)),
            dma((nz, nx)),
            dma((nz,)),
            dma((nz,)),
        ],
        compiler_params=pltpu.CompilerParams(
            collective_id=ident, has_side_effects=True, vmem_limit_bytes=48 * 1024 * 1024
        ),
    )(partial.reshape(nz, nx, nc, rows, width), mid)


def shards(
    plan,
    resid_in,
    query_latent,
    kv_latent,
    rotary_key,
    query_gain,
    kv_gain,
    w_query_plain,
    w_query_rotary,
    w_key_plain,
    w_value,
    w_output,
    ffn_gain,
    w_gate,
    w_up,
    w_down,
):
    tok, width = resid_in.shape
    heads_dev = w_query_plain.shape[1] // NOPE
    nz = plan.z
    hidden_dev = w_gate.shape[1]
    part = min(-(-hidden_dev // (nz * 128)) * 128, hidden_dev)

    offset = lax.axis_index("sp") * tok
    position = (offset + jnp.arange(tok, dtype=jnp.int32)).astype(jnp.float32)
    freq = 10000.0 ** (-jnp.arange(0, ROPE, 2, dtype=jnp.float32) / ROPE)
    angle = position[:, None] * freq[None, :]
    cosine = jnp.cos(angle)
    sine = jnp.sin(angle)
    kv_norm = normed(kv_latent, kv_gain).astype(jnp.bfloat16)
    key_rot = rotate(rotary_key.astype(jnp.float32), cosine, sine).astype(jnp.bfloat16)
    piece = tok // plan.c
    packed = lax.dynamic_slice_in_dim(
        jnp.concatenate([kv_norm, key_rot], axis=1),
        lax.rem(lax.axis_index("tp"), plan.c) * piece,
        piece,
        0,
    )
    q_norm = normed(query_latent, query_gain).astype(jnp.bfloat16)
    q_plain = (
        jnp.dot(q_norm, w_query_plain, preferred_element_type=jnp.float32)
        .astype(jnp.bfloat16)
    )
    q_raw = jnp.dot(q_norm, w_query_rotary, preferred_element_type=jnp.float32).reshape(
        tok, heads_dev, ROPE
    )
    q_rot = rotate(q_raw, cosine[:, None, :], sine[:, None, :]).astype(jnp.bfloat16)
    share = tok // plan.tp
    own_start = lax.axis_index("tp") * share
    mid, h_norm, both, down = front(
        plan,
        heads_dev,
        part,
        packed,
        q_plain,
        jnp.transpose(q_rot, (1, 0, 2)),
        w_key_plain,
        w_value,
        w_output,
        lax.dynamic_slice_in_dim(resid_in, own_start, share, 0),
        ffn_gain[None, :],
        w_gate,
        w_up,
        w_down,
        1,
    )
    if down.ndim == 3:
        down = jnp.transpose(down, (1, 0, 2)).reshape(part, width)
    inner = jnp.dot(h_norm.reshape(-1, width), both, preferred_element_type=jnp.float32)
    place = lax.axis_index("sp") // plan.r * part
    lane = lax.broadcasted_iota(jnp.int32, (1, part), 1)
    fresh = lane >= place - jnp.minimum(place, hidden_dev - part)
    hidden = jnp.where(fresh, jax.nn.silu(inner[:, :part]) * inner[:, part:], 0.0)
    partial = jnp.dot(hidden.astype(jnp.bfloat16), down, preferred_element_type=jnp.float32)
    return reduce_add(plan, partial.astype(jnp.bfloat16), mid, 2)


def solution(mesh):
    plan = Plan(mesh.shape["sp"], mesh.shape["tp"])
    return jax.shard_map(
        functools.partial(shards, plan),
        mesh=mesh,
        in_specs=(
            P("sp", None),
            P("sp", None),
            P("sp", None),
            P("sp", None),
            P(),
            P(),
            P(None, "tp"),
            P(None, "tp"),
            P(None, "tp"),
            P(None, "tp"),
            P("tp", None),
            P(),
            P("sp", "tp"),
            P("sp", "tp"),
            P("tp", "sp"),
        ),
        out_specs=P(("sp", "tp"), None),
        check_vma=False,
    )
```

profile of v0, /device:TPU:0, one launch (start us, length us, event | category | flops | bytes accessed | tf_op | source)
XLA Modules:
  0.0 168.0 jit_solution(6382561101984655124)
XLA Ops:
  0.0 0.0 copy-start
  0.0 0.0 copy-start.2
  0.0 0.0 copy-start.6
  0.0 1.2 fusion.9
  1.2 1.2 fusion.2
  2.4 0.0 copy-start.4
  2.4 0.9 copy.20
  3.4 0.0 copy-start.5
  3.4 0.6 multiply_cosine_fusion
  4.0 1.1 fusion.11
  5.1 0.8 fusion.13.kv_ref
  5.8 0.0 copy-done
  5.8 0.7 constant_dynamic-slice_fusion.resid_ref
  6.5 0.0 copy-done.2
  6.5 0.0 copy-done.6
  6.6 0.0 copy-done.5
  6.6 0.4 fusion.14
  7.0 0.0 copy-done.4
  7.0 1.1 convolution_convert_fusion.1.qp_ref
  8.1 0.2 copy.25
  8.3 0.2 copy.24
  8.5 0.1 subtract_convert_fusion
  8.7 0.8 maximum_bitcast_fusion.qr_ref
  9.5 107.8 %shard_map.145 = (f32[64,2048]{1,0:T(8,128)}, bf16[16,64,2048]{2,1,0:T(8,128)(2,1)}, bf16[2048,768]{1,0:T(8,128)(2,1)}, bf16[384,2048]{1,0:T(8,128)(2,1)}) custom-call(bf16[128,576]{1,0:T(8,128)(2,1)} %fusion.13.kv_ref, bf16[256,512]{1,0:T(8,128)(2,1)} %convolution_convert_fusion.1.qp_ref, bf16[4,256,64]{2,1,0:T(8,128)(2,1)} %maximum_bitcast_fusion.qr_ref, ...), custom_call_target="tpu_custom_call" | custom-call | tf_op jit(solution)/shard_map/pallas_call | solution.py:326
  117.3 0.0 copy-start.3
  117.3 6.2 %fusion.20 = f32[1024,768]{1,0:T(8,128)S(1)} fusion(bf16[1024,2048]{1,0:T(8,128)(2,1)} %bitcast.14, bf16[2048,768]{1,0:T(8,128)(2,1)} %get-tuple-element.10), kind=kOutput, calls=%fused_computation.40 | convolution fusion | flops 3221225472 | bytes 10485760 | tf_op jit(solution)/shard_map/dot_general | solution.py:543
  123.6 0.0 copy-done.3
  123.6 0.0 copy-start.1
  123.6 2.4 %convolution_convert_fusion = bf16[1024,2048]{1,0:T(8,128)(2,1)S(1)} fusion(bf16[384,2048]{1,0:T(8,128)(2,1)S(1)} %copy-done.3, f32[1024,768]{1,0:T(8,128)S(1)} %fusion.20, pred[384]{0:T(512)(128)(4,1)S(1)} %iota_compare_fusion), kind=kOutput, calls=%fused_computation | convolution fusion | flops 1615462400 | bytes 8913280 | tf_op jit(solution)/shard_map/dot_general | solution.py:548
  126.0 0.0 copy-done.1
  126.0 41.3 %shard_map.146 = bf16[64,2048]{1,0:T(8,128)(2,1)S(1)} custom-call(bf16[4,2,2,64,2048]{4,3,2,1,0:T(8,128)(2,1)S(1)} %bitcast.11, f32[64,2048]{1,0:T(8,128)S(1)} %copy-done.1), custom_call_target="tpu_custom_call" | custom-call | tf_op jit(solution)/shard_map/pallas_call | solution.py:450
  167.3 0.7 copy.27
  (7 shorter events, 0.1 us)
Async XLA Ops:
  0.0 5.8 %copy-start = (bf16[256,2048]{1,0:T(8,128)(2,1)S(1)}, bf16[256,2048]{1,0:T(8,128)(2,1)}, u32[]{:S(2)}) copy-start(bf16[256,2048]{1,0:T(8,128)(2,1)} %param.15) | copy-start | bytes 3145732
  0.0 6.5 %copy-start.2 = (bf16[256,768]{1,0:T(8,128)(2,1)S(1)}, bf16[256,768]{1,0:T(8,128)(2,1)}, u32[]{:S(2)}) copy-start(bf16[256,768]{1,0:T(8,128)(2,1)} %param.16) | copy-start | bytes 1179652
  0.0 6.5 %copy-start.6 = (f32[768]{0:T(1024)S(1)}, f32[768]{0:T(1024)}, u32[]{:S(2)}) copy-start(f32[768]{0:T(1024)} %param.19) | copy-start | bytes 9220
  2.4 4.6 %copy-start.4 = (bf16[768,512]{1,0:T(8,128)(2,1)S(1)}, bf16[768,512]{1,0:T(8,128)(2,1)}, u32[]{:S(2)}) copy-start(bf16[768,512]{1,0:T(8,128)(2,1)} %param.21) | copy-start | bytes 2359300
  3.4 3.2 %copy-start.5 = (bf16[768,256]{1,0:T(8,128)(2,1)S(1)}, bf16[768,256]{1,0:T(8,128)(2,1)}, u32[]{:S(2)}) copy-start(bf16[768,256]{1,0:T(8,128)(2,1)} %param.22) | copy-start | bytes 1179652
  117.3 6.3 %copy-start.3 = (bf16[384,2048]{1,0:T(8,128)(2,1)S(1)}, bf16[384,2048]{1,0:T(8,128)(2,1)}, u32[]{:S(2)}) copy-start(bf16[384,2048]{1,0:T(8,128)(2,1)} %get-tuple-element.11) | copy-start | bytes 4718596
  123.6 2.4 %copy-start.1 = (f32[64,2048]{1,0:T(8,128)S(1)}, f32[64,2048]{1,0:T(8,128)}, u32[]{:S(2)}) copy-start(f32[64,2048]{1,0:T(8,128)} %get-tuple-element.12.m_ref) | copy-start | bytes 1572868
where the time goes:
time: 168 us
  Pallas kernels  149 us (89%)
  matrix products  10.1 us (6%)
  other arithmetic  5.8 us (3%)
  local copies, waits for them, and re-layouts  2.8 us (2%)
    pallas_call x1, Pallas kernels, front(): pl.pallas_call(functools.partial(front_body, plan, heads, part), out_shap...  108 us
    pallas_call x1, Pallas kernels, reduce_add(): pl.pallas_call(functools.partial(reduce_body, plan), out_shape=jax.ShapeD...  41.3 us
    dot_general x1, matrix products, shards(): jnp.dot(h_norm.reshape(-1, width), both, preferred_element_type=jnp.float32)  6.25 us

commit v1 on v0

--- a/solution.py
+++ b/solution.py
@@ -48,22 +48,6 @@
     def shifted(self, at, axis, by):
         size = self.sizes()[axis]
         return {**at, axis: lax.rem(at[axis] + (by % size), size)}
-
-
-def meet(plan, here, axes):
-    barrier = pltpu.get_barrier_semaphore()
-    count = 0
-    for axis in axes:
-        for k in range(1, plan.sizes()[axis]):
-            pl.semaphore_signal(
-                barrier,
-                inc=1,
-                device_id=plan.device(plan.shifted(here, axis, k)),
-                device_id_type=MESH,
-            )
-            count += 1
-    if count:
-        pl.semaphore_wait(barrier, count)
 
 
 def front_body(
@@ -81,6 +65,7 @@
     gate_ref,
     up_ref,
     down_ref,
+    o_ref,
     mid_ref,
     hn_ref,
     both_ref,
@@ -90,6 +75,12 @@
     out,
     terms,
     h_own,
+    part_ref,
+    got_c,
+    sum_c,
+    got_x,
+    sum_x,
+    got_z,
     kv_sa,
     kv_ra,
     kv_sb,
@@ -108,6 +99,12 @@
     w_rb,
     t_s,
     t_r,
+    c_s,
+    c_r,
+    x_s,
+    x_r,
+    z_s,
+    z_r,
     local,
 ):
     here = plan.here()
@@ -169,31 +166,33 @@
             for k in range(1, sizes[self.axes[0]]):
                 self.send(0, here, k, ())
 
-        def run(self):
-            na, nb, nc = (sizes[axis] for axis in self.axes)
-            for k in range(na):
+        def relay(self, k):
+            block = plan.shifted(here, self.axes[0], -k)
+            if k:
+                self.copies[(k,)].wait_recv()
+            for j in range(1, sizes[self.axes[1]]):
+                self.send(1, block, j, (k,))
+            for l in range(1, sizes[self.axes[2]]):
+                self.send(2, block, l, (k, 0))
+
+        def relay_on(self, k):
+            for j in range(1, sizes[self.axes[1]]):
+                self.copies[(k, j)].wait_recv()
                 block = plan.shifted(here, self.axes[0], -k)
-                if k:
-                    self.copies[(k,)].wait_recv()
-                for j in range(1, nb):
-                    self.send(1, block, j, (k,))
-                for l in range(1, nc):
-                    self.send(2, block, l, (k, 0))
-            for k in range(na):
-                for j in range(1, nb):
-                    self.copies[(k, j)].wait_recv()
-                    block = plan.shifted(here, self.axes[0], -k)
-                    block = plan.shifted(block, self.axes[1], -j)
-                    for l in range(1, nc):
-                        self.send(2, block, l, (k, j))
+                block = plan.shifted(block, self.axes[1], -j)
+                for l in range(1, sizes[self.axes[2]]):
+                    self.send(2, block, l, (k, j))
+
+        def landed(self, k):
+            if k == 0:
+                self.mine.wait()
+            for key, copy in self.copies.items():
+                if len(key) == 3 and key[0] == k:
+                    copy.wait_recv()
 
         def finish(self):
-            for key, copy in self.copies.items():
-                if len(key) == 3:
-                    copy.wait_recv()
             for copy in self.copies.values():
                 copy.wait_send()
-            self.mine.wait()
 
     def window(index):
         return pl.multiple_of(jnp.minimum(index * part, full - part), 128)
@@ -227,7 +226,10 @@
             over_z[w, k] = send(
                 sources(to["z"])[w], dst, plan.device(to), w_sa.at[w, k], w_ra.at[w, k]
             )
-    kv.run()
+    for k in range(nz):
+        kv.relay(k)
+    for k in range(nz):
+        kv.relay_on(k)
 
     def forward(w, k):
         block = plan.shifted(here, "z", -k)
@@ -246,7 +248,8 @@
 
     for w in range(3):
         forward(w, 0)
-    kv.finish()
+    for k in range(nz):
+        kv.landed(k)
 
     scale = (NOPE + ROPE) ** (-0.5)
     count = packed.shape[0] * packed.shape[1]
@@ -295,18 +298,102 @@
     ).astype(jnp.bfloat16)
     hn = Gather(("z", "x", "c"), h_own, hn_ref, (hn_sa, hn_ra, hn_sb, hn_rb, hn_sc, hn_rc), local.at[1])
     hn.start()
+    hn.relay(0)
     for k in range(1, nz):
         forward(2, k)
-    hn.run()
+    for copy in over_r.values():
+        copy.wait_recv()
+    for copy in mine:
+        copy.wait()
+
+    nx, nc = plan.x, plan.c
+    x, c = here["x"], here["c"]
+    place = here["z"] * part
+    lane = lax.broadcasted_iota(jnp.int32, (1, part), 1)
+    fresh = lane >= place - jnp.minimum(place, full - part)
+    wide = jnp.float32
+    over_c, over_x, back = {}, {}, {}
+
+    def feed(k):
+        first = plan.shifted(here, "z", -k)["z"] * tp
+        rows = hn_ref[pl.ds(first, tp)].reshape(tp * share, -1)
+        inner = jnp.dot(rows, both_ref[...], preferred_element_type=wide)
+        hidden = jnp.where(fresh, jax.nn.silu(inner[:, :part]) * inner[:, part:], 0.0)
+        hidden = hidden.astype(jnp.bfloat16)
+        if len(downs_ref.shape) == 3:
+            for i in range(downs_ref.shape[0]):
+                piece = jnp.dot(hidden, downs_ref[i], preferred_element_type=wide)
+                part_ref[k, :, :, :, i * narrow : (i + 1) * narrow] = piece.astype(
+                    jnp.bfloat16
+                ).reshape(nx, nc, share, narrow)
+        else:
+            piece = jnp.dot(hidden, downs_ref[...], preferred_element_type=wide)
+            part_ref[k] = piece.astype(jnp.bfloat16).reshape(nx, nc, share, -1)
+        for l in range(1, nc):
+            for i in range(nx):
+                over_c[k, i, l] = send(
+                    part_ref.at[k, i, lax.rem(c + l, nc)],
+                    got_c.at[k, i, l - 1],
+                    plan.device(plan.shifted(here, "c", l)),
+                    c_s.at[k, i, l],
+                    c_r.at[k, i, l],
+                )
+
+    def fold_c(k):
+        for i in range(nx):
+            total = part_ref[k, i, c].astype(wide)
+            for l in range(1, nc):
+                over_c[k, i, l].wait_recv()
+                total += got_c[k, i, l - 1].astype(wide)
+            sum_c[k, i] = total.astype(jnp.bfloat16)
+        for j in range(1, nx):
+            over_x[k, j] = send(
+                sum_c.at[k, lax.rem(x + j, nx)],
+                got_x.at[k, j - 1],
+                plan.device(plan.shifted(here, "x", j)),
+                x_s.at[k, j],
+                x_r.at[k, j],
+            )
+
+    def fold_x(k):
+        total = sum_c[k, x].astype(wide)
+        for j in range(1, nx):
+            over_x[k, j].wait_recv()
+            total += got_x[k, j - 1].astype(wide)
+        if k == 0:
+            mid_ref[...] += total
+            return
+        sum_x[k - 1] = total.astype(jnp.bfloat16)
+        back[k] = send(
+            sum_x.at[k - 1],
+            got_z.at[k - 1],
+            plan.device(plan.shifted(here, "z", -k)),
+            z_s.at[k],
+            z_r.at[k],
+        )
+
+    for k in range(nz):
+        if k + 1 < nz:
+            hn.relay(k + 1)
+        hn.relay_on(k)
+        hn.landed(k)
+        feed(k)
+        if k:
+            fold_x(k - 1)
+        fold_c(k)
+    fold_x(nz - 1)
+    total = mid_ref[...]
+    for k in range(1, nz):
+        back[k].wait_recv()
+        total += got_z[k - 1].astype(wide)
+    o_ref[...] = total.astype(jnp.bfloat16)
+    kv.finish()
     hn.finish()
+    for copies in (over_z, over_r, over_c, over_x, back):
+        for copy in copies.values():
+            copy.wait_send()
     for copy in swaps:
         copy.wait_send()
-    for copy in over_r.values():
-        copy.wait_recv()
-    for copy in [*over_z.values(), *over_r.values()]:
-        copy.wait_send()
-    for copy in mine:
-        copy.wait()
 
 
 def front(plan, heads, part, kv, qp, qr, wk, wv, wo, resid, gain, gate, up, down, ident):
@@ -315,7 +402,6 @@
     tok = qp.shape[0]
     dma = pltpu.SemaphoreType.DMA
     vmem = pl.BlockSpec(memory_space=pltpu.VMEM)
-    hbm = pl.BlockSpec(memory_space=pl.ANY)
 
     def sems(a, b, c):
         return [dma((a,)), dma((a,)), dma((a, b)), dma((a, b)), dma((a, b, c)), dma((a, b, c))]
@@ -325,20 +411,25 @@
     downs = (part, plan.sp * narrow) if narrow % 128 == 0 else (plan.sp, part, narrow)
     return pl.pallas_call(
         functools.partial(front_body, plan, heads, part),
-        out_shape=(
-            jax.ShapeDtypeStruct((share, width), jnp.float32),
-            jax.ShapeDtypeStruct((nz * tp, share, width), bf),
-            jax.ShapeDtypeStruct((plan.sp * gate.shape[0], 2 * part), bf),
-            jax.ShapeDtypeStruct(downs, bf),
-        ),
+        out_shape=jax.ShapeDtypeStruct((share, width), bf),
         in_specs=[vmem] * 11,
-        out_specs=(vmem, hbm, hbm, hbm),
+        out_specs=vmem,
         scratch_shapes=[
+            pltpu.VMEM((share, width), jnp.float32),
+            pltpu.VMEM((nz * tp, share, width), bf),
+            pltpu.VMEM((plan.sp * gate.shape[0], 2 * part), bf),
+            pltpu.VMEM(downs, bf),
             pltpu.VMEM((nz * nr * nc,) + kv.shape, bf),
             pltpu.VMEM((tok, heads * VDIM), bf),
             pltpu.VMEM((tp, share, width), bf),
             pltpu.VMEM((tp, share, width), bf),
             pltpu.VMEM((share, width), bf),
+            pltpu.VMEM((nz, nx, nc, share, width), bf),
+            pltpu.VMEM((nz, nx, max(nc - 1, 1), share, width), bf),
+            pltpu.VMEM((nz, nx, share, width), bf),
+            pltpu.VMEM((nz, max(nx - 1, 1), share, width), bf),
+            pltpu.VMEM((max(nz - 1, 1), share, width), bf),
+            pltpu.VMEM((max(nz - 1, 1), share, width), bf),
             *sems(nz, nr, nc),
             *sems(nz, nx, nc),
             dma((3, nz)),
@@ -347,128 +438,18 @@
             dma((3, nz, nr)),
             dma((tp,)),
             dma((tp,)),
-            dma((5,)),
-        ],
-        compiler_params=pltpu.CompilerParams(
-            collective_id=ident, has_side_effects=True, vmem_limit_bytes=56 * 1024 * 1024
-        ),
-    )(kv, qp, qr, wk, wv, wo, resid, gain, gate, up, down)
-
-
-def reduce_body(
-    plan, p_ref, m_ref, o_ref, got_c, sum_c, got_x, sum_x, got_z, s_c, r_c, s_x, r_x, s_z, r_z
-):
-    nz, nx, nc = plan.z, plan.x, plan.c
-    here = plan.here()
-    z, x, c = here["z"], here["x"], here["c"]
-    meet(plan, here, ("z", "x", "c"))
-
-    def send(src, dst, axis, by, sem_s, sem_r):
-        copy = pltpu.make_async_remote_copy(
-            src_ref=src,
-            dst_ref=dst,
-            send_sem=sem_s,
-            recv_sem=sem_r,
-            device_id=plan.device(plan.shifted(here, axis, by)),
-            device_id_type=MESH,
-        )
-        copy.start()
-        return copy
-
-    def wide(value):
-        return value.astype(jnp.float32)
-
-    steps = [k for k in (2, 1, 3) if k < nz] + [0]
-    if nz != 4:
-        steps = list(range(1, nz)) + [0]
-    over_c, over_x, over_z = {}, {}, {}
-    for k in steps:
-        to = lax.rem(z + k, nz)
-        for l in range(1, nc):
-            other = lax.rem(c + l, nc)
-            for i in range(nx):
-                over_c[k, i, l] = send(
-                    p_ref.at[to, i, other],
-                    got_c.at[k, i, l - 1],
-                    "c",
-                    l,
-                    s_c.at[k, i, l],
-                    r_c.at[k, i, l],
-                )
-
-    def fold_c(k):
-        to = lax.rem(z + k, nz)
-        for i in range(nx):
-            total = wide(p_ref[to, i, c])
-            for l in range(1, nc):
-                over_c[k, i, l].wait_recv()
-                total += wide(got_c[k, i, l - 1])
-            sum_c[k, i] = total.astype(jnp.bfloat16)
-        for j in range(1, nx):
-            over_x[k, j] = send(
-                sum_c.at[k, lax.rem(x + j, nx)],
-                got_x.at[k, j - 1],
-                "x",
-                j,
-                s_x.at[k, j],
-                r_x.at[k, j],
-            )
-
-    def fold_x(k):
-        total = wide(sum_c[k, x])
-        for j in range(1, nx):
-            over_x[k, j].wait_recv()
-            total += wide(got_x[k, j - 1])
-        if k:
-            sum_x[k - 1] = total.astype(jnp.bfloat16)
-            over_z[k] = send(sum_x.at[k - 1], got_z.at[k - 1], "z", k, s_z.at[k], r_z.at[k])
-            return None
-        return total
-
-    for k in steps:
-        fold_c(k)
-    for k in steps:
-        total = fold_x(k)
-    for k in steps:
-        if k:
-            over_z[k].wait_recv()
-            total += wide(got_z[k - 1])
-    o_ref[...] = (m_ref[...] + total).astype(jnp.bfloat16)
-    for copy in [*over_c.values(), *over_x.values(), *over_z.values()]:
-        copy.wait_send()
-
-
-def reduce_add(plan, partial, mid, ident):
-    nz, nx, nc = plan.z, plan.x, plan.c
-    rows, width = mid.shape
-    dma = pltpu.SemaphoreType.DMA
-
-    def buf(*lead):
-        return pltpu.VMEM(lead + (rows, width), jnp.bfloat16)
-
-    vmem = pl.BlockSpec(memory_space=pltpu.VMEM)
-    return pl.pallas_call(
-        functools.partial(reduce_body, plan),
-        out_shape=jax.ShapeDtypeStruct(mid.shape, jnp.bfloat16),
-        in_specs=[vmem, vmem],
-        out_specs=vmem,
-        scratch_shapes=[
-            buf(nz, nx, max(nc - 1, 1)),
-            buf(nz, nx),
-            buf(nz, max(nx - 1, 1)),
-            buf(max(nz - 1, 1)),
-            buf(max(nz - 1, 1)),
             dma((nz, nx, nc)),
             dma((nz, nx, nc)),
             dma((nz, nx)),
             dma((nz, nx)),
             dma((nz,)),
             dma((nz,)),
+            dma((5,)),
         ],
         compiler_params=pltpu.CompilerParams(
-            collective_id=ident, has_side_effects=True, vmem_limit_bytes=48 * 1024 * 1024
+            collective_id=ident, has_side_effects=True, vmem_limit_bytes=62 * 1024 * 1024
         ),
-    )(partial.reshape(nz, nx, nc, rows, width), mid)
+    )(kv, qp, qr, wk, wv, wo, resid, gain, gate, up, down)
 
 
 def shards(
@@ -489,7 +470,7 @@
     w_up,
     w_down,
 ):
-    tok, width = resid_in.shape
+    tok = resid_in.shape[0]
     heads_dev = w_query_plain.shape[1] // NOPE
     nz = plan.z
     hidden_dev = w_gate.shape[1]
@@ -521,7 +502,7 @@
     q_rot = rotate(q_raw, cosine[:, None, :], sine[:, None, :]).astype(jnp.bfloat16)
     share = tok // plan.tp
     own_start = lax.axis_index("tp") * share
-    mid, h_norm, both, down = front(
+    return front(
         plan,
         heads_dev,
         part,
@@ -538,15 +519,6 @@
         w_down,
         1,
     )
-    if down.ndim == 3:
-        down = jnp.transpose(down, (1, 0, 2)).reshape(part, width)
-    inner = jnp.dot(h_norm.reshape(-1, width), both, preferred_element_type=jnp.float32)
-    place = lax.axis_index("sp") // plan.r * part
-    lane = lax.broadcasted_iota(jnp.int32, (1, part), 1)
-    fresh = lane >= place - jnp.minimum(place, hidden_dev - part)
-    hidden = jnp.where(fresh, jax.nn.silu(inner[:, :part]) * inner[:, part:], 0.0)
-    partial = jnp.dot(hidden.astype(jnp.bfloat16), down, preferred_element_type=jnp.float32)
-    return reduce_add(plan, partial.astype(jnp.bfloat16), mid, 2)
 
 
 def solution(mesh):

time: 168 us -> 160 us (0.952)
  matrix products: 10.1 us -> 2.66 us
    pallas_call x1 -> x0, Pallas kernels: 41.3 us -> none  [reduce_add(): pl.pallas_call(functools.partial(reduce_body, plan), out_shape=jax.ShapeD...]
    pallas_call x1, Pallas kernels: 108 us -> 149 us  [front(): pl.pallas_call(functools.partial(front_body, plan, heads, part), out_shap...]
    dot_general x2 -> x0, matrix products: 8.6 us -> none  [the longest x1 6.25 us: shards(): jnp.dot(h_norm.reshape(-1, width), both, preferred_element_type=jnp.float32)]
where the time goes in v1:
time: 160 us
  Pallas kernels  149 us (93%)
  other arithmetic  4.7 us (3%)
  local copies, waits for them, and re-layouts  3.8 us (2%)
  matrix products  2.66 us (2%)
    pallas_call x1, Pallas kernels, front(): pl.pallas_call(functools.partial(front_body, plan, heads, part), out_shap...  149 us

profile of v1, /device:TPU:0, one launch (start us, length us, event | category | flops | bytes accessed | tf_op | source)
XLA Modules:
  0.0 160.1 jit_solution(6544037353635735548)
XLA Ops:
  0.0 0.0 copy-start
  0.0 0.0 copy-start.1
  0.0 0.0 copy-start.3
  0.0 0.0 copy-start.2
  0.0 1.0 copy.20
  1.1 0.6 multiply_cosine_fusion
  1.7 1.1 fusion.3
  2.8 1.1 fusion.5
  3.8 0.8 fusion.7.kv_ref
  4.6 0.0 copy-done.1
  4.6 0.2 fusion
  4.8 0.0 copy-done.3
  4.8 0.0 copy-done.2
  4.8 0.4 fusion.8
  5.2 0.2 copy.24
  5.4 0.2 copy.25
  5.6 0.2 subtract_convert_fusion
  5.8 0.8 maximum_bitcast_fusion.qr_ref
  6.6 0.0 copy-done
  6.6 0.7 constant_dynamic-slice_fusion.resid_ref
  7.4 2.3 %convolution_convert_fusion.qp_ref = bf16[256,512]{1,0:T(8,128)(2,1)} fusion(bf16[768,512]{1,0:T(8,128)(2,1)} %param.21, bf16[256,768]{1,0:T(8,128)(2,1)S(1)} %copy-done.1, f32[768]{0:T(1024)S(1)} %copy-done.3, f32[256]{0:T(256)S(1)} %add_rsqrt_fusion), kind=kOutput, calls=%fused_computation | convolution fusion | flops 202244096 | bytes 1445888 | tf_op jit(solution)/shard_map/dot_general | solution.py:496
  9.6 148.8 %shard_map.145 = bf16[64,2048]{1,0:T(8,128)(2,1)} custom-call(bf16[128,576]{1,0:T(8,128)(2,1)} %fusion.7.kv_ref, bf16[256,512]{1,0:T(8,128)(2,1)} %convolution_convert_fusion.qp_ref, bf16[4,256,64]{2,1,0:T(8,128)(2,1)} %maximum_bitcast_fusion.qr_ref, bf16[512,512]{1,0:T(8,128)(2,1)} %wk_ref.1, bf16[512,512]{1,0:T(8,128)(2,1)} %wv_ref.1, ...), custom_call_target="tpu_custom_call" | custom-call | tf_op jit(solution)/shard_map/pallas_call | solution.py:412
  158.4 1.7 %copy.27 = bf16[64,2048]{1,0:T(8,128)(2,1)} copy(bf16[64,2048]{1,0:T(8,128)(2,1)} %shard_map.145) | data formatting | bytes 524288
  (6 shorter events, 0.1 us)
Async XLA Ops:
  0.0 6.6 %copy-start = (bf16[256,2048]{1,0:T(8,128)(2,1)S(1)}, bf16[256,2048]{1,0:T(8,128)(2,1)}, u32[]{:S(2)}) copy-start(bf16[256,2048]{1,0:T(8,128)(2,1)} %param.15) | copy-start | bytes 3145732
  0.0 4.6 %copy-start.1 = (bf16[256,768]{1,0:T(8,128)(2,1)S(1)}, bf16[256,768]{1,0:T(8,128)(2,1)}, u32[]{:S(2)}) copy-start(bf16[256,768]{1,0:T(8,128)(2,1)} %param.16) | copy-start | bytes 1179652
  0.0 4.8 %copy-start.3 = (f32[768]{0:T(1024)S(1)}, f32[768]{0:T(1024)}, u32[]{:S(2)}) copy-start(f32[768]{0:T(1024)} %param.19) | copy-start | bytes 9220
  0.0 4.8 %copy-start.2 = (bf16[768,256]{1,0:T(8,128)(2,1)S(1)}, bf16[768,256]{1,0:T(8,128)(2,1)}, u32[]{:S(2)}) copy-start(bf16[768,256]{1,0:T(8,128)(2,1)} %param.22) | copy-start | bytes 1179652

commit v2 on v1

--- a/solution.py
+++ b/solution.py
@@ -273,6 +273,8 @@
         mixed = jnp.dot(weight.astype(jnp.bfloat16), vals, preferred_element_type=jnp.float32)
         attn[:, lanes] = (mixed / total).astype(jnp.bfloat16)
 
+    for k in range(1, nz):
+        forward(0, k)
     share = out.shape[1]
     swaps = []
     for k in list(range(1, tp)) + [0]:
@@ -285,9 +287,8 @@
             swaps.append(
                 send(out.at[to], terms.at[k], {"sp": sp_here, "tp": to}, t_s.at[k], t_r.at[k])
             )
-    for w in range(2):
-        for k in range(1, nz):
-            forward(w, k)
+    for k in range(1, nz):
+        forward(1, k)
     mid = resid_ref[...].astype(jnp.float32) + out[tp_here].astype(jnp.float32)
     for k, copy in enumerate(swaps, 1):
         copy.wait_recv()
@@ -373,9 +374,9 @@
         )
 
     for k in range(nz):
+        hn.relay_on(k)
         if k + 1 < nz:
             hn.relay(k + 1)
-        hn.relay_on(k)
         hn.landed(k)
         feed(k)
         if k:

time: 160 us -> 160 us (level)
  no operation moved by 1% of the time
where the time goes in v2:
time: 160 us; the launch traced here: 159 us
  Pallas kernels  148 us (92%)
  other arithmetic  4.7 us (3%)
  local copies, waits for them, and re-layouts  3.8 us (2%)
  matrix products  2.66 us (2%)
    pallas_call x1, Pallas kernels, front(): pl.pallas_call(functools.partial(front_body, plan, heads, part), out_shap...  148 us

profile of v2, /device:TPU:0, one launch (start us, length us, event | category | flops | bytes accessed | tf_op | source)
XLA Modules:
  0.0 159.3 jit_solution(9742077233646482310)
XLA Ops:
  0.0 0.0 copy-start
  0.0 0.0 copy-start.1
  0.0 0.0 copy-start.3
  0.0 0.0 copy-start.2
  0.0 1.0 copy.20
  1.1 0.6 multiply_cosine_fusion
  1.7 1.1 fusion.3
  2.8 1.1 fusion.5
  3.8 0.8 fusion.7.kv_ref
  4.6 0.0 copy-done.1
  4.6 0.2 fusion
  4.8 0.0 copy-done.3
  4.8 0.0 copy-done.2
  4.8 0.4 fusion.8
  5.2 0.2 copy.24
  5.4 0.2 copy.25
  5.6 0.2 subtract_convert_fusion
  5.8 0.8 maximum_bitcast_fusion.qr_ref
  6.6 0.0 copy-done
  6.6 0.7 constant_dynamic-slice_fusion.resid_ref
  7.4 2.3 %convolution_convert_fusion.qp_ref = bf16[256,512]{1,0:T(8,128)(2,1)} fusion(bf16[768,512]{1,0:T(8,128)(2,1)} %param.21, bf16[256,768]{1,0:T(8,128)(2,1)S(1)} %copy-done.1, f32[768]{0:T(1024)S(1)} %copy-done.3, f32[256]{0:T(256)S(1)} %add_rsqrt_fusion), kind=kOutput, calls=%fused_computation | convolution fusion | flops 202244096 | bytes 1445888 | tf_op jit(solution)/shard_map/dot_general | solution.py:497
  9.6 148.0 %shard_map.145 = bf16[64,2048]{1,0:T(8,128)(2,1)} custom-call(bf16[128,576]{1,0:T(8,128)(2,1)} %fusion.7.kv_ref, bf16[256,512]{1,0:T(8,128)(2,1)} %convolution_convert_fusion.qp_ref, bf16[4,256,64]{2,1,0:T(8,128)(2,1)} %maximum_bitcast_fusion.qr_ref, bf16[512,512]{1,0:T(8,128)(2,1)} %wk_ref.1, bf16[512,512]{1,0:T(8,128)(2,1)} %wv_ref.1, ...), custom_call_target="tpu_custom_call" | custom-call | tf_op jit(solution)/shard_map/pallas_call | solution.py:413
  157.6 1.7 %copy.27 = bf16[64,2048]{1,0:T(8,128)(2,1)} copy(bf16[64,2048]{1,0:T(8,128)(2,1)} %shard_map.145) | data formatting | bytes 524288
  (6 shorter events, 0.1 us)
Async XLA Ops:
  0.0 6.6 %copy-start = (bf16[256,2048]{1,0:T(8,128)(2,1)S(1)}, bf16[256,2048]{1,0:T(8,128)(2,1)}, u32[]{:S(2)}) copy-start(bf16[256,2048]{1,0:T(8,128)(2,1)} %param.15) | copy-start | bytes 3145732
  0.0 4.6 %copy-start.1 = (bf16[256,768]{1,0:T(8,128)(2,1)S(1)}, bf16[256,768]{1,0:T(8,128)(2,1)}, u32[]{:S(2)}) copy-start(bf16[256,768]{1,0:T(8,128)(2,1)} %param.16) | copy-start | bytes 1179652
  0.0 4.8 %copy-start.3 = (f32[768]{0:T(1024)S(1)}, f32[768]{0:T(1024)}, u32[]{:S(2)}) copy-start(f32[768]{0:T(1024)} %param.19) | copy-start | bytes 9220
  0.0 4.8 %copy-start.2 = (bf16[768,256]{1,0:T(8,128)(2,1)S(1)}, bf16[768,256]{1,0:T(8,128)(2,1)}, u32[]{:S(2)}) copy-start(bf16[768,256]{1,0:T(8,128)(2,1)} %param.22) | copy-start | bytes 1179652
